TPU v7x, 32 devices: a whole 2x2x4 slice. The times are simulated.
32 devices in a mesh: rep: 2 (over x), fs: 4 (over z), tp: 4 (over y, core).
Axes of the slice: x: 2, y: 2, z: 4, core: 2. Of those that a mesh axis runs over, the one named last changes fastest.
Arguments:
- tokens: bfloat16 [8192, 2048], P(('rep', 'fs'), 'tp'), may hold values from -6 to 6
- mix_in_gain: bfloat16 [2048], replicated, may hold values from 0.099609375 to 1.8984375
- bgate_weight: bfloat16 [2048, 2048], P('fs', 'tp'), may hold values from -0.125 to 0.125
- cgate_weight: bfloat16 [2048, 2048], P('fs', 'tp'), may hold values from -0.125 to 0.125
- value_weight: bfloat16 [2048, 2048], P('fs', 'tp'), may hold values from -0.125 to 0.125
- conv_taps: bfloat16 [3, 2048], replicated, may hold values from -3 to 3
- out_weight: bfloat16 [2048, 2048], P('tp', 'fs'), may hold values from -0.41984465 to 0.41984465
- mix_out_gain: bfloat16 [2048], replicated, may hold values from 0.099609375 to 1.8984375
- ffn_in_gain: bfloat16 [2048], replicated, may hold values from 0.099609375 to 1.8984375
- up_weight: bfloat16 [2048, 8192], P('fs', 'tp'), may hold values from -0.125 to 0.125
- down_weight: bfloat16 [8192, 2048], P('tp', 'fs'), may hold values from -0.20992233 to 0.20992233
- ffn_out_gain: bfloat16 [2048], replicated, may hold values from 0.099609375 to 1.8984375
Outputs:
- result: bfloat16 [8192, 2048], P(('rep', 'fs'), 'tp')
All inputs are finite; a program needn't handle non-finite values.
Results may differ from a plain program's by a relative error of at most 0.02.
Values may be sent and summed in bfloat16 or wider, within the bound.
A program may use at most 128 MiB of HBM per device.

v0:
```python
import jax
import jax.numpy as jnp
from jax import lax
from jax.sharding import PartitionSpec as P

LEN = 256


epsilon = 1e-06


def normalize(rows, gain):
    rows = rows.astype(jnp.float32)
    factor = lax.rsqrt(jnp.mean(rows * rows, axis=-1, keepdims=True) + epsilon)
    return rows * factor * gain.astype(jnp.float32)


def convolve(inner, taps):
    seqs = inner.reshape(-1, LEN, inner.shape[1])
    padded = jnp.pad(seqs, ((0, 0), (1, 1), (0, 0)))
    weights = taps.astype(jnp.float32)
    out = weights[0] * padded[:, :-2] + weights[1] * padded[:, 1:-1] + weights[2] * padded[:, 2:]
    return out.reshape(inner.shape)


def body(
    tokens,
    mix_in_gain,
    bgate_weight,
    cgate_weight,
    value_weight,
    conv_taps,
    out_weight,
    mix_out_gain,
    ffn_in_gain,
    up_weight,
    down_weight,
    ffn_out_gain,
):
    column = lax.axis_index("tp")
    own_width = tokens.shape[1]
    first = column * own_width
    full_width = mix_in_gain.shape[0]
    whole = lax.all_gather(tokens, "tp", axis=1, tiled=True)
    normed = normalize(whole, mix_in_gain).astype(jnp.bfloat16)

    def add_rows(piece):
        return jnp.dot(normed, piece, preferred_element_type=jnp.float32)

    bgate = add_rows(lax.all_gather(bgate_weight, "fs", axis=0, tiled=True))
    cgate = add_rows(lax.all_gather(cgate_weight, "fs", axis=0, tiled=True))
    value = add_rows(lax.all_gather(value_weight, "fs", axis=0, tiled=True))
    bgate = bgate.astype(jnp.bfloat16)
    cgate = cgate.astype(jnp.bfloat16)
    value = value.astype(jnp.bfloat16)
    channels = bgate.shape[1]
    own_taps = lax.dynamic_slice_in_dim(conv_taps, column * channels, channels, 1)
    inner = cgate.astype(jnp.float32) * value.astype(jnp.float32)
    gated = (bgate.astype(jnp.float32) * convolve(inner, own_taps)).astype(jnp.bfloat16)
    partial_mix = jnp.dot(
        gated,
        lax.all_gather(out_weight, "fs", axis=1, tiled=True),
        preferred_element_type=jnp.float32,
    )
    mixed = lax.psum(partial_mix.astype(jnp.bfloat16), "tp").astype(jnp.float32)
    resid = (whole.astype(jnp.float32) + normalize(mixed, mix_out_gain)).astype(jnp.bfloat16)
    resid_own = lax.dynamic_slice_in_dim(resid, first, own_width, 1)
    second = normalize(resid, ffn_in_gain).astype(jnp.bfloat16)
    lifted = jnp.dot(
        second,
        lax.all_gather(up_weight, "fs", axis=0, tiled=True),
        preferred_element_type=jnp.float32,
    )
    active = jnp.square(jnp.maximum(lifted, 0.0)).astype(jnp.bfloat16)
    partial_ffn = jnp.dot(
        active,
        lax.all_gather(down_weight, "fs", axis=1, tiled=True),
        preferred_element_type=jnp.float32,
    )
    ffn = lax.psum_scatter(
        partial_ffn.astype(jnp.bfloat16), "tp", scatter_dimension=1, tiled=True
    ).astype(jnp.float32)
    ffn_energy = lax.psum(jnp.sum(ffn * ffn, axis=1), "tp")
    out_gain = lax.dynamic_slice_in_dim(ffn_out_gain, first, own_width, 0).astype(jnp.float32)
    closing = ffn * lax.rsqrt(ffn_energy[:, None] / full_width + epsilon) * out_gain
    return (resid_own.astype(jnp.float32) + closing).astype(jnp.bfloat16)


def solution(mesh):
    placed = (
        P(("rep", "fs"), "tp"),
        P(),
        P("fs", "tp"),
        P("fs", "tp"),
        P("fs", "tp"),
        P(),
        P("tp", "fs"),
        P(),
        P(),
        P("fs", "tp"),
        P("tp", "fs"),
        P(),
    )
    return jax.shard_map(
        body, mesh=mesh, in_specs=placed, out_specs=P(("rep", "fs"), "tp"), check_vma=False
    )
```

profile of v0, /device:TPU:0, one launch (start us, length us, event | category | flops | bytes accessed | tf_op | source)
XLA Modules:
  0.0 707.6 jit_solution(8818610116150277627)
XLA Ops:
  6.5 0.7 all-gather.8.cloned.1.call-update
  7.3 0.7 all-gather.12.cloned.1.call-update
  8.1 0.7 all-gather.14.cloned.1.call-update
  8.8 0.5 all-gather.10.cloned.1.call-update
  9.4 0.5 all-gather.16.cloned.1.call-update
  10.0 0.7 dynamic-slice_convert_fusion
  10.7 0.7 convert_element_type.76
  11.4 34.8 %all-gather.8.cloned.1.call-done = bf16[1024,2048]{1,0:T(8,128)(2,1)} async-done(((bf16[1024,512]{1,0:T(8,128)(2,1)}), bf16[1024,2048]{1,0:T(8,128)(2,1)}) %all-gather.8.cloned.1.call-update) | async-done | bytes 4194320 | tf_op jit(solution)/shard_map/all_gather | solution.py:44
  46.1 3.1 fusion.5
  49.2 44.2 %all-gather.12.cloned.1.call-done = bf16[2048,512]{1,0:T(8,128)(2,1)} async-done(((bf16[512,512]{1,0:T(8,128)(2,1)}), bf16[2048,512]{1,0:T(8,128)(2,1)}) %all-gather.12.cloned.1.call-update) | async-done | bytes 2097168 | tf_op jit(solution)/shard_map/all_gather | solution.py:51
  93.4 5.2 convolution_convert_fusion.2
  98.6 40.8 %all-gather.14.cloned.1.call-done = bf16[2048,512]{1,0:T(8,128)(2,1)} async-done(((bf16[512,512]{1,0:T(8,128)(2,1)}), bf16[2048,512]{1,0:T(8,128)(2,1)}) %all-gather.14.cloned.1.call-update) | async-done | bytes 2097168 | tf_op jit(solution)/shard_map/all_gather | solution.py:52
  139.4 5.2 convert_multiply_fusion.8
  144.7 0.6 multiply_add_fusion
  145.3 40.0 %all-gather.10.cloned.1.call-done = bf16[2048,512]{1,0:T(8,128)(2,1)} async-done(((bf16[512,512]{1,0:T(8,128)(2,1)}), bf16[2048,512]{1,0:T(8,128)(2,1)}) %all-gather.10.cloned.1.call-update) | async-done | bytes 2097168 | tf_op jit(solution)/shard_map/all_gather | solution.py:50
  185.4 5.2 fusion.25
  190.6 40.7 %all-gather.16.cloned.1.call-done = bf16[512,2048]{1,0:T(8,128)(2,1)} async-done(((bf16[512,512]{1,0:T(8,128)(2,1)}), bf16[512,2048]{1,0:T(8,128)(2,1)}) %all-gather.16.cloned.1.call-update) | async-done | bytes 2097168 | tf_op jit(solution)/shard_map/all_gather | solution.py:62
  231.3 5.9 convolution_convert_fusion
  237.2 0.7 all-gather.18.cloned.1.call-update
  238.0 0.7 all-gather.20.cloned.1.call-update
  238.7 0.2 reduce-scatter.2.cloned.1.call-start
  239.0 82.7 %all-reduce.3.cloned.1.call-done = bf16[1024,2048]{1,0:T(8,128)(2,1)} async-done(((bf16[1024,2048]{1,0:T(8,128)(2,1)}), bf16[1024,2048]{1,0:T(8,128)(2,1)}) %all-reduce.3.cloned.1.call-update) | async-done | bytes 4194320 | tf_op jit(solution)/shard_map/psum | solution.py:65
  321.6 3.2 fusion
  325.1 5.3 fusion.2
  330.4 142.6 %all-gather.18.cloned.1.call-done = bf16[2048,2048]{1,0:T(8,128)(2,1)} async-done(((bf16[512,2048]{1,0:T(8,128)(2,1)}), bf16[2048,2048]{1,0:T(8,128)(2,1)}) %all-gather.18.cloned.1.call-update) | async-done | bytes 8388624 | tf_op jit(solution)/shard_map/all_gather | solution.py:71
  473.0 149.4 %all-gather.20.cloned.1.call-done = bf16[2048,2048]{1,0:T(8,128)(2,1)} async-done(((bf16[2048,512]{1,0:T(8,128)(2,1)}), bf16[2048,2048]{1,0:T(8,128)(2,1)}) %all-gather.20.cloned.1.call-update) | async-done | bytes 8388624 | tf_op jit(solution)/shard_map/all_gather | solution.py:77
  622.4 25.7 %fusion.18 = bf16[1024,2048]{1,0:T(8,128)(2,1)} fusion(bf16[2048,2048]{1,0:T(8,128)(2,1)} %all-gather.20.cloned.1.call-done, bf16[2048,2048]{1,0:T(8,128)(2,1)} %all-gather.18.cloned.1.call-done, bf16[1024,2048]{1,0:T(8,128)(2,1)} %get-tuple-element.6, f32[2048]{0:T(1024)S(1)} %convert_element_type.92, f32[1024]{0:T(1024)S(1)} %add_rsqrt_fusion.1), kind=kOutput, calls=%fused_computation.22 | convolution fusion | flops 17196646400 | bytes 25178112 | tf_op jit(solution)/shard_map/dot_general | solution.py:75
  648.1 0.8 dynamic-slice_convert_fusion.1
  648.8 41.9 %reduce-scatter.2.cloned.1.call-done = bf16[1024,512]{1,0:T(8,128)(2,1)} async-done(((bf16[1024,2048]{1,0:T(8,128)(2,1)}), bf16[1024,512]{1,0:T(8,128)(2,1)}) %reduce-scatter.2.cloned.1.call-update) | async-done | bytes 1048592 | tf_op jit(solution)/shard_map/reduce_scatter | solution.py:80
  690.8 1.5 fusion.21
  692.3 5.8 psum.15
  698.1 3.0 fusion.24
  (23 shorter events, 0.6 us)
Async XLA Ops:
  6.5 39.6 %all-gather.8.cloned.1.call-start = ((), (), s32[]{:S(2)}) async-start(), calls=%async_computation.1 | async-start | bytes 5242880 | tf_op jit(solution)/shard_map/all_gather | solution.py:44
  7.3 86.1 %all-gather.12.cloned.1.call-start = ((), (), s32[]{:S(2)}) async-start(), calls=%async_computation.3 | async-start | bytes 2621440 | tf_op jit(solution)/shard_map/all_gather | solution.py:51
  8.0 131.4 %all-gather.14.cloned.1.call-start = ((), (), s32[]{:S(2)}) async-start(), calls=%async_computation.4 | async-start | bytes 2621440 | tf_op jit(solution)/shard_map/all_gather | solution.py:52
  8.7 176.6 %all-gather.10.cloned.1.call-start = ((), (), s32[]{:S(2)}) async-start(), calls=%async_computation.2 | async-start | bytes 2621440 | tf_op jit(solution)/shard_map/all_gather | solution.py:50
  9.3 221.9 %all-gather.16.cloned.1.call-start = ((), (), s32[]{:S(2)}) async-start(), calls=%async_computation.5 | async-start | bytes 2621440 | tf_op jit(solution)/shard_map/all_gather | solution.py:62
  9.9 311.7 %all-reduce.3.cloned.1.call-start = ((), (), s32[]{:S(2)}) async-start(), calls=%async_computation.6 | async-start | bytes 8388608 | tf_op jit(solution)/shard_map/psum | solution.py:65
  237.2 1.8 copy-start.1
  237.2 1.8 copy-start.2
  237.2 235.8 %all-gather.18.cloned.1.call-start = ((), (), s32[]{:S(2)}) async-start(), calls=%async_computation.7 | async-start | bytes 10485760 | tf_op jit(solution)/shard_map/all_gather | solution.py:71
  237.9 384.4 %all-gather.20.cloned.1.call-start = ((), (), s32[]{:S(2)}) async-start(), calls=%async_computation.8 | async-start | bytes 10485760 | tf_op jit(solution)/shard_map/all_gather | solution.py:77
  238.7 452.1 %reduce-scatter.2.cloned.1.call-start = ((), (), s32[]{:S(2)}) async-start(), calls=%async_computation.9 | async-start | bytes 5242880 | tf_op jit(solution)/shard_map/reduce_scatter | solution.py:80
  321.6 3.4 copy-start
Sparse Core Ops, SparseCore 0:
  8.9 37.1 all-gather.7
  47.7 45.6 all-gather.11
  94.9 44.4 all-gather.13
  140.9 44.4 all-gather.9
  186.8 44.4 all-gather.15
  237.3 84.2 all-reduce.2
  323.2 149.7 all-gather.17
  474.6 147.7 all-gather.19
  648.2 42.5 reduce-scatter.1
where the time goes:
time: 708 us
  waiting for transfers between devices  622 us (88%)
  matrix products  47.3 us (7%)
  other arithmetic  18.9 us (3%)
  between operations  13.3 us (2%)
    all_gather x1, waiting for transfers between devices, body(): lax.all_gather(down_weight, 'fs', axis=1, tiled=True)  149 us
    all_gather x1, waiting for transfers between devices, body(): lax.all_gather(up_weight, 'fs', axis=0, tiled=True)  143 us
    psum x1, waiting for transfers between devices, body(): mixed = lax.psum(partial_mix.astype(jnp.bfloat16), 'tp').astype(jnp.float32)  82.7 us
    all_gather x1, waiting for transfers between devices, body(): cgate = add_rows(lax.all_gather(cgate_weight, 'fs', axis=0, tiled=True))  44.2 us
    reduce_scatter x1, waiting for transfers between devices, body(): lax.psum_scatter(partial_ffn.astype(jnp.bfloat16), 'tp', scatter_dimensio...  41.9 us
    all_gather x1, waiting for transfers between devices, body(): value = add_rows(lax.all_gather(value_weight, 'fs', axis=0, tiled=True))  40.8 us
    all_gather x1, waiting for transfers between devices, body(): lax.all_gather(out_weight, 'fs', axis=1, tiled=True)  40.7 us
    all_gather x1, waiting for transfers between devices, body(): bgate = add_rows(lax.all_gather(bgate_weight, 'fs', axis=0, tiled=True))  40 us
  transfers between devices with their start and end apart: 9, of which 9 were waited for; matrix products, arithmetic and copies ran while one was open for 4% of the time, Pallas kernels for 0%

commit v1 on v0

v1 whole, which is shorter than its diff:
```python
import functools

import jax
import jax.numpy as jnp
from jax import lax
from jax.experimental import pallas as pl
from jax.experimental.pallas import tpu as pltpu
from jax.sharding import PartitionSpec as P

LEN = 256
LANES = 128
AHEAD = 3

epsilon = 1e-06
MESH = pl.DeviceIdType.MESH
F32 = jnp.float32
BF16 = jnp.bfloat16


def at(index, size):
    return pl.ds(pl.multiple_of(index * size, size), size)


def dot(left, right):
    return jnp.dot(left, right, preferred_element_type=F32)


def kernel(
    nfs, ntp, nu, nc, cw,
    tokens, gain1, wb, wc, wv, taps, wo, gain2, gain3, wu, wd, gain4,
    result,
    rows_w, out_w, down_w, tok, normed, part, rs, mix, active, energy,
    recv_z, recv_x, send_r, send_l, send_x, local_sem, tok_local,
    tok_send, tok_recv, rs_send, rs_recv, ag_send, ag_recv, ff_send, ff_recv, en_send, en_recv,
):
    rep, fs, tp = lax.axis_index("rep"), lax.axis_index("fs"), lax.axis_index("tp")
    count, own = tokens.shape
    width = own * ntp
    seqs = count // LEN
    krows = wb.shape[0]
    chan = wb.shape[1]
    ucol = wu.shape[1] // nu
    ocol = wo.shape[1]
    nk = 3 + 1 + nu + nc
    first_down = 4 + nu

    barrier = pltpu.get_barrier_semaphore()
    for step in (1, nfs - 1):
        pl.semaphore_signal(barrier, inc=1, device_id={"fs": lax.rem(fs + step, nfs)}, device_id_type=MESH)
    pl.semaphore_signal(barrier, inc=1, device_id={"rep": 1 - rep}, device_id_type=MESH)
    for step in range(1, ntp):
        pl.semaphore_signal(barrier, inc=1, device_id={"tp": lax.rem(tp + step, ntp)}, device_id_type=MESH)
    pl.semaphore_wait(barrier, 3 + ntp - 1)

    def region(k, s, half):
        if k < 3 or 4 <= k < first_down:
            index = k if k < 3 else k - 1
            if half is None:
                return rows_w.at[index, at(s, krows), :]
            return rows_w.at[index, at(s * 2 + half, krows // 2), :]
        if k == 3:
            r = slice(None) if half is None else at(half, wo.shape[0] // 2)
            return out_w.at[r, at(s, ocol)]
        r = slice(None) if half is None else at(half, wd.shape[0] // 2)
        return down_w.at[k - first_down, r, at(s, cw)]

    def source(k, half):
        if k < 3:
            ref, c = (wb, wc, wv)[k], slice(None)
        elif k == 3:
            ref, c = wo, slice(None)
        elif k < first_down:
            ref, c = wu, pl.ds((k - 4) * ucol, ucol)
        else:
            ref, c = wd, pl.ds((k - first_down) * cw, cw)
        r = slice(None) if half is None else at(half, ref.shape[0] // 2)
        return ref.at[r, c]

    def hop(k, s, src, sems, to):
        return pltpu.make_async_remote_copy(
            src, region(k, s, rep), sems.at[k, s], recv_z.at[k, s],
            device_id={"fs": to}, device_id_type=MESH)

    def right(k, s, src=None):
        return hop(k, s, region(k, s, rep) if src is None else src, send_r, lax.rem(fs + 1, nfs))

    def left(k, s, src=None):
        return hop(k, s, region(k, s, rep) if src is None else src, send_l, lax.rem(fs + nfs - 1, nfs))

    def across(k, s, half):
        return pltpu.make_async_remote_copy(
            region(k, s, half), region(k, s, half), send_x.at[k, s], recv_x.at[k, s],
            device_id={"rep": 1 - rep}, device_id_type=MESH)

    def send_own(k):
        @pl.when(fs < nfs - 1)
        def _():
            right(k, fs, source(k, rep)).start()

        @pl.when(fs > 0)
        def _():
            left(k, fs, source(k, rep)).start()

    def local(k):
        return pltpu.make_async_copy(source(k, None), region(k, fs, None), local_sem.at[k])

    def advance(k):
        if k + AHEAD < nk:
            send_own(k + AHEAD)

        def one(d, carry):
            @pl.when(fs - d >= 0)
            def _():
                s = fs - d
                right(k, s).wait_recv()

                @pl.when(fs < nfs - 1)
                def _():
                    right(k, s).start()

                across(k, s, rep).start()

            @pl.when(fs + d < nfs)
            def _():
                s = fs + d
                left(k, s).wait_recv()

                @pl.when(fs > 0)
                def _():
                    left(k, s).start()

                across(k, s, rep).start()

            return carry

        lax.fori_loop(1, nfs, one, 0)

    def complete(k):
        def one(s, carry):
            @pl.when(s != fs)
            def _():
                across(k, s, 1 - rep).wait_recv()

            return carry

        lax.fori_loop(0, nfs, one, 0)
        local(k).wait()

    def drain(k):
        def one(s, carry):
            @pl.when((s <= fs) & (fs < nfs - 1))
            def _():
                right(k, s).wait_send()

            @pl.when((s >= fs) & (fs > 0))
            def _():
                left(k, s).wait_send()

            @pl.when(s != fs)
            def _():
                across(k, s, rep).wait_send()

            return carry

        lax.fori_loop(0, nfs, one, 0)

    def group(t, src, dst, send, recv):
        return pltpu.make_async_remote_copy(
            src, dst, send, recv,
            device_id={"tp": lax.rem(tp + t, ntp)}, device_id_type=MESH)

    def tok_copy(t):
        mine = tok.at[:, at(tp, own)]
        return group(t, tokens, mine, tok_send.at[t - 1], tok_recv.at[t - 1])

    def rs_copy(t):
        to = lax.rem(tp + t, ntp)
        return group(t, part.at[:, at(to, own)], rs.at[t - 1], rs_send.at[t - 1], rs_recv.at[t - 1])

    def ag_copy(t):
        mine = mix.at[:, at(tp, own)]
        return group(t, mine, mine, ag_send.at[t - 1], ag_recv.at[t - 1])

    block = nfs * cw
    piece = block // ntp

    def ff_copy(t, c):
        to = lax.rem(tp + t, ntp)
        src = part.at[:, at(c * ntp + to, piece)]
        return group(t, src, rs.at[t - 1, :, pl.ds(c * piece, piece)], ff_send.at[t - 1, c], ff_recv.at[t - 1, c])

    def en_copy(t):
        return group(t, energy.at[0], energy.at[t], en_send.at[t - 1], en_recv.at[t - 1])

    def each_seq(fn):
        def one(i, carry):
            fn(at(i, LEN))
            return carry

        lax.fori_loop(0, seqs, one, 0)

    def factor(v):
        return lax.rsqrt(jnp.mean(v * v, axis=-1, keepdims=True) + epsilon)

    send_own(0)
    for t in range(1, ntp):
        tok_copy(t).start()
    own_tok = pltpu.make_async_copy(tokens, tok.at[:, at(tp, own)], tok_local)
    own_tok.start()
    for k in range(1, AHEAD):
        send_own(k)
    for k in range(nk):
        local(k).start()

    advance(0)
    advance(1)
    own_tok.wait()
    for t in range(1, ntp):
        tok_copy(t).wait_recv()

    def norm_tokens(r):
        v = tok[r, :].astype(F32)
        normed[r, :] = (v * factor(v) * gain1[...].astype(F32)).astype(BF16)

    each_seq(norm_tokens)
    advance(2)
    advance(3)
    for k in range(3):
        complete(k)

    own_taps = taps[:, at(tp, chan)].astype(F32)
    position = lax.broadcasted_iota(jnp.int32, (LEN, chan), 0)

    def mixer(r):
        rows = normed[r, :]
        inner = dot(rows, rows_w[1]).astype(BF16).astype(F32) * dot(rows, rows_w[2]).astype(BF16).astype(F32)
        before = jnp.where(position == 0, 0.0, pltpu.roll(inner, 1, 0))
        after = jnp.where(position == LEN - 1, 0.0, pltpu.roll(inner, LEN - 1, 0))
        conv = own_taps[0:1] * before + own_taps[1:2] * inner + own_taps[2:3] * after
        outer = dot(rows, rows_w[0]).astype(BF16).astype(F32)
        active[r, 0:chan] = (outer * conv).astype(BF16)

    each_seq(mixer)
    advance(4)
    complete(3)

    def project(r):
        part[r, :] = dot(active[r, 0:chan], out_w[...]).astype(BF16)

    each_seq(project)
    for t in range(1, ntp):
        rs_copy(t).start()
    done = 5
    for k in range(done, min(first_down, nk)):
        advance(k)
    for t in range(1, ntp):
        rs_copy(t).wait_recv()

    def add_mix(r):
        total = part[r, at(tp, own)].astype(F32)
        for t in range(1, ntp):
            total = total + rs[t - 1, r, :].astype(F32)
        mix[r, at(tp, own)] = total.astype(BF16)

    each_seq(add_mix)
    for t in range(1, ntp):
        ag_copy(t).start()
    early = max(nc - 2, 0)
    for c in range(early):
        advance(first_down + c)
    for k in range(4, first_down):
        complete(k)
    for t in range(1, ntp):
        ag_copy(t).wait_recv()

    def second(r):
        m = mix[r, :].astype(F32)
        res = (tok[r, :].astype(F32) + m * factor(m) * gain2[...].astype(F32)).astype(BF16)
        tok[r, :] = res
        res = res.astype(F32)
        rows = (res * factor(res) * gain3[...].astype(F32)).astype(BF16)
        for u in range(nu):
            lifted = jnp.maximum(dot(rows, rows_w[3 + u]), 0.0)
            active[r, pl.ds(u * ucol, ucol)] = (lifted * lifted).astype(BF16)

    for t in range(1, ntp):
        tok_copy(t).wait_send()
        rs_copy(t).wait_send()
    each_seq(second)

    for c in range(nc):
        if early <= c + 1 < nc:
            advance(first_down + c + 1)
        if c == 0 and early == 0:
            advance(first_down)
        complete(first_down + c)

        def down(r):
            part[r, pl.ds(c * block, block)] = dot(active[r, :], down_w[c]).astype(BF16)

        each_seq(down)
        for t in range(1, ntp):
            ff_copy(t, c).start()

    for k in range(nk):
        drain(k)
    for t in range(1, ntp):
        ag_copy(t).wait_send()
        for c in range(nc):
            ff_copy(t, c).wait_recv()

    def own_ffn(r):
        pieces = [part[r, at(c * ntp + tp, piece)] for c in range(nc)]
        total = (pieces[0] if nc == 1 else jnp.concatenate(pieces, axis=1)).astype(F32)
        for t in range(1, ntp):
            total = total + rs[t - 1, r, :].astype(F32)
        return total

    def measure(r):
        total = own_ffn(r)
        square = jnp.sum(total * total, axis=1, keepdims=True)
        flat = jnp.transpose(jnp.broadcast_to(square, (LEN, LANES)))
        energy[0, :, r] = flat[0:8, :]

    each_seq(measure)
    for t in range(1, ntp):
        en_copy(t).start()
    for t in range(1, ntp):
        en_copy(t).wait_recv()
    own_gain = gain4[:, at(tp, own)].astype(F32)

    def close(r):
        total = own_ffn(r)
        flat = energy[0, :, r]
        for t in range(1, ntp):
            flat = flat + energy[t, :, r]
        tall = jnp.transpose(jnp.concatenate([flat] * (LANES // 8), axis=0))
        scale = lax.rsqrt(tall[:, 0:1] / width + epsilon)
        result[r, :] = (tok[r, at(tp, own)].astype(F32) + total * scale * own_gain).astype(BF16)

    each_seq(close)
    for t in range(1, ntp):
        en_copy(t).wait_send()
        for c in range(nc):
            ff_copy(t, c).wait_send()


def solution(mesh):
    nfs, ntp = mesh.shape["fs"], mesh.shape["tp"]
    assert mesh.shape["rep"] == 2

    def body(tokens, gain1, wb, wc, wv, taps, wo, gain2, gain3, wu, wd, gain4):
        count, own = tokens.shape
        width, chan, hidden = own * ntp, wb.shape[1], wu.shape[1]
        ucol = chan
        nu = hidden // ucol
        cw = min(LANES, wd.shape[1])
        nc = wd.shape[1] // cw
        nk = 4 + nu + nc
        vm, anyw = pl.BlockSpec(memory_space=pltpu.VMEM), pl.BlockSpec(memory_space=pl.ANY)
        dma = pltpu.SemaphoreType.DMA
        peers = ntp - 1
        return pl.pallas_call(
            functools.partial(kernel, nfs, ntp, nu, nc, cw),
            out_shape=jax.ShapeDtypeStruct((count, own), BF16),
            in_specs=[anyw, vm, anyw, anyw, anyw, vm, anyw, vm, vm, anyw, anyw, vm],
            out_specs=vm,
            scratch_shapes=[
                pltpu.VMEM((3 + nu, width, chan), BF16),
                pltpu.VMEM((chan, width), BF16),
                pltpu.VMEM((nc, hidden, nfs * cw), BF16),
                pltpu.VMEM((count, width), BF16),
                pltpu.VMEM((count, width), BF16),
                pltpu.VMEM((count, width), BF16),
                pltpu.VMEM((peers, count, own), BF16),
                pltpu.VMEM((count, width), BF16),
                pltpu.VMEM((count, hidden), BF16),
                pltpu.VMEM((ntp, 8, count), F32),
                dma((nk, nfs)), dma((nk, nfs)), dma((nk, nfs)), dma((nk, nfs)), dma((nk, nfs)),
                dma((nk,)), dma,
                dma((peers,)), dma((peers,)), dma((peers,)), dma((peers,)),
                dma((peers,)), dma((peers,)), dma((peers, nc)), dma((peers, nc)),
                dma((peers,)), dma((peers,)),
            ],
            compiler_params=pltpu.CompilerParams(
                collective_id=0, has_side_effects=True, vmem_limit_bytes=64000000),
            name="layer",
        )(tokens, gain1[None], wb, wc, wv, taps, wo, gain2[None], gain3[None], wu, wd, gain4[None])

    placed = (
        P(("rep", "fs"), "tp"), P(), P("fs", "tp"), P("fs", "tp"), P("fs", "tp"), P(), P("tp", "fs"),
        P(), P(), P("fs", "tp"), P("tp", "fs"), P(),
    )
    return jax.shard_map(
        body, mesh=mesh, in_specs=placed, out_specs=P(("rep", "fs"), "tp"), check_vma=False
    )
```

time: 708 us -> 270 us (0.38)
  waiting for transfers between devices: 622 us -> 0 us
  Pallas kernels: 0 us -> 262 us
  matrix products: 47.3 us -> 0 us
  other arithmetic: 18.9 us -> 0 us
  between operations: 13.3 us -> 0.01 us
  local copies, waits for them, and re-layouts: 0.23 us -> 7.41 us
    all_gather x7 -> x0, waiting for transfers between devices: 492 us -> none  [the longest x1 149 us: body(): lax.all_gather(down_weight, 'fs', axis=1, tiled=True)]
    pallas_call x0 -> x1, Pallas kernels: none -> 262 us  [body(): pl.pallas_call(functools.partial(kernel, nfs, ntp, nu, nc, cw), out_shape...]
    psum x1 -> x0, waiting for transfers between devices: 82.7 us -> none  [body(): mixed = lax.psum(partial_mix.astype(jnp.bfloat16), 'tp').astype(jnp.float32)]
    dot_general x5 -> x0, matrix products: 47.3 us -> none  [the longest x1 25.7 us: body(): jnp.dot(active, lax.all_gather(down_weight, 'fs', axis=1, tiled=True), pr...]
    reduce_scatter x1 -> x0, waiting for transfers between devices: 41.9 us -> none  [body(): lax.psum_scatter(partial_ffn.astype(jnp.bfloat16), 'tp', scatter_dimensio...]
    reduce_sum x4 -> x0, other arithmetic: 13.1 us -> none  [the longest x3 11.6 us: normalize(): factor = lax.rsqrt(jnp.mean(rows * rows, axis=-1, keepdims=True) + epsilon)]
  transfers between devices with their start and end apart: 9 -> 0, of which waited for: 9 -> 0; matrix products, arithmetic and copies ran while one was open for 4% -> 0% of each run, Pallas kernels for 0% -> 0%
where the time goes in v1:
time: 270 us; the launch traced here: 269 us
  Pallas kernels  262 us (97%)
  local copies, waits for them, and re-layouts  7.41 us (3%)
    pallas_call x1, Pallas kernels, body(): pl.pallas_call(functools.partial(kernel, nfs, ntp, nu, nc, cw), out_shape...  262 us

profile of v1, /device:TPU:0, one launch (start us, length us, event | category | flops | bytes accessed | tf_op | source)
XLA Modules:
  0.0 269.4 jit_solution(9301001691929092865)
XLA Ops:
  0.0 1.3 broadcast_in_dim.12.gain1
  1.3 1.3 broadcast_in_dim.13.gain2
  2.6 1.3 broadcast_in_dim.14.gain3
  3.9 1.3 broadcast_in_dim.15.gain4
  5.1 261.9 %layer.1 = bf16[1024,512]{1,0:T(8,128)(2,1)} custom-call(bf16[1024,512]{1,0:T(8,128)(2,1)} %tokens.1, bf16[1,2048]{1,0:T(2,128)(2,1)} %broadcast_in_dim.12.gain1, bf16[512,512]{1,0:T(8,128)(2,1)} %wb.1, bf16[512,512]{1,0:T(8,128)(2,1)} %wc.1, bf16[512,512]{1,0:T(8,128)(2,1)} %wv.1, bf16[3,2048]{1,0:T(4,128)(2,1)} %taps.1, bf16[512,512]{1,0:T(8,128)(2,1)} %wo.1, ...), custom_call_target="tpu_custom_call" | custom-call | tf_op jit(solution)/shard_map/layer/pallas_call | solution.py:363
  267.1 2.3 copy.14

commit v2 on v1

--- a/solution.py
+++ b/solution.py
@@ -9,7 +9,7 @@
 
 LEN = 256
 LANES = 128
-AHEAD = 3
+AHEAD = 1
 
 epsilon = 1e-06
 MESH = pl.DeviceIdType.MESH

time: 270 us -> 256 us (0.948)
  Pallas kernels: 262 us -> 249 us
    pallas_call x1, Pallas kernels: 262 us -> 249 us  [body(): pl.pallas_call(functools.partial(kernel, nfs, ntp, nu, nc, cw), out_shape...]
where the time goes in v2:
time: 256 us
  Pallas kernels  249 us (97%)
  local copies, waits for them, and re-layouts  7.41 us (3%)
    pallas_call x1, Pallas kernels, body(): pl.pallas_call(functools.partial(kernel, nfs, ntp, nu, nc, cw), out_shape...  249 us

profile of v2, /device:TPU:0, one launch (start us, length us, event | category | flops | bytes accessed | tf_op | source)
XLA Modules:
  0.0 256.1 jit_solution(12055334470951717921)
XLA Ops:
  0.0 1.3 broadcast_in_dim.12.gain1
  1.3 1.3 broadcast_in_dim.13.gain2
  2.6 1.3 broadcast_in_dim.14.gain3
  3.9 1.3 broadcast_in_dim.15.gain4
  5.1 248.7 %layer.1 = bf16[1024,512]{1,0:T(8,128)(2,1)} custom-call(bf16[1024,512]{1,0:T(8,128)(2,1)} %tokens.1, bf16[1,2048]{1,0:T(2,128)(2,1)} %broadcast_in_dim.12.gain1, bf16[512,512]{1,0:T(8,128)(2,1)} %wb.1, bf16[512,512]{1,0:T(8,128)(2,1)} %wc.1, bf16[512,512]{1,0:T(8,128)(2,1)} %wv.1, bf16[3,2048]{1,0:T(4,128)(2,1)} %taps.1, bf16[512,512]{1,0:T(8,128)(2,1)} %wo.1, ...), custom_call_target="tpu_custom_call" | custom-call | tf_op jit(solution)/shard_map/layer/pallas_call | solution.py:363
  253.8 2.3 copy.14
